TPU v7x, 32 devices: a whole 2x2x4 slice. The times are simulated.
32 devices in a mesh: sp: 8 (over z, core), tp: 4 (over y, x).
Axes of the slice: x: 2, y: 2, z: 4, core: 2. Of those that a mesh axis runs over, the one named last changes fastest.
Arguments:
- residual_in: bfloat16 [2048, 2048], P(('sp', 'tp')), may hold values from -6 to 6
- query_a: bfloat16 [2048, 1024], P('sp', 'tp'), may hold values from -12 to 12
- key_a: bfloat16 [2048, 1024], P('sp', 'tp'), may hold values from -12 to 12
- value_a: bfloat16 [2048, 1024], P('sp', 'tp'), may hold values from -6 to 6
- query_b: bfloat16 [2048, 2048], P('sp', 'tp'), may hold values from -12 to 12
- key_b: bfloat16 [2048, 2048], P('sp', 'tp'), may hold values from -12 to 12
- value_b: bfloat16 [2048, 2048], P('sp', 'tp'), may hold values from -6 to 6
- cum_gates: float32 [2048, 2, 16], P('sp', None, 'tp'), may hold values from -247.76 to 0, as said below
- out_a: bfloat16 [1024, 2048], P('tp'), may hold values from -0.1875 to 0.1875
- out_b: bfloat16 [2048, 2048], P('tp'), may hold values from -0.125 to 0.125
- post_gain: bfloat16 [2048], replicated, may hold values from 0.099609375 to 1.8984375
- pre_gain: bfloat16 [2048], replicated, may hold values from 0.099609375 to 1.8984375
- expert_ids: int32 [2048, 2], P('sp'), may hold values from 0 to 7, all different within a row; in each aligned block of 256 rows (0 to 255, 256 to 511, ...) at most 80 rows name the same one
- expert_weights: float32 [2048, 2], P('sp'), may hold values from 0.2 to 1
- w_gate: bfloat16 [8, 2048, 4096], P('sp', None, 'tp'), may hold values from -0.125 to 0.125
- w_up: bfloat16 [8, 2048, 4096], P('sp', None, 'tp'), may hold values from -0.125 to 0.125
- w_down: bfloat16 [8, 4096, 2048], P('sp', 'tp'), may hold values from -0.09375 to 0.09375
Outputs:
- layer_out: bfloat16 [2048, 2048], P(('sp', 'tp'))
Inputs may be any that keep to these rules, and one draw needn't show every extreme that they name: `expert_ids`: in each aligned block of 256 positions no expert is named by more than 80 routes, a bound that some block reaches; a token's experts differ. `cum_gates`: never rises along the positions.
All inputs are finite; a program needn't handle non-finite values.
Results may differ from a plain program's by a relative error of at most 0.015.
Values may be sent and summed in bfloat16 or wider, within the bound.
A program may use at most 64 MiB of HBM per device.

v0:
```python
import jax
import jax.numpy as jnp
from jax import lax
from jax.sharding import PartitionSpec as P

eps_norm = 1e-06
big_neg = -1e30


def rms_scale(values, gain):
    return values * lax.rsqrt(jnp.mean(values * values, axis=-1, keepdims=True) + eps_norm) * gain


def empty_state(item_count, heads, width):
    return (
        jnp.full((heads, item_count), big_neg, jnp.float32),
        jnp.zeros((heads, item_count), jnp.float32),
        jnp.zeros((heads, item_count, width), jnp.float32),
    )


def update_state(state, query, key_rows, values, query_gate, key_gate, mask, width):
    highest, total, accum = state
    score = jnp.einsum(
        "rhd,khd->hrk", query, key_rows, preferred_element_type=jnp.float32
    ) * width ** (-0.5)
    score = score + query_gate.T[:, :, None] - key_gate.T[:, None, :]
    new_high = jnp.maximum(highest, jnp.max(jnp.where(mask[None], score, big_neg), axis=2))
    expo = jnp.exp(jnp.where(mask[None], score - new_high[:, :, None], big_neg))
    total = jnp.sum(expo, axis=2)
    accum = jnp.einsum(
        "hrk,khd->hrd", expo.astype(jnp.bfloat16), values, preferred_element_type=jnp.float32
    )
    return (new_high, total, accum)


def finish(state):
    highest, total, accum = state
    heads, item_count, width = accum.shape
    result = accum / total[:, :, None]
    return result.transpose(1, 0, 2).reshape(item_count, heads * width).astype(jnp.bfloat16)


def per_device(
    residual_in,
    query_a,
    key_a,
    value_a,
    query_b,
    key_b,
    value_b,
    cum_gates,
    out_a,
    out_b,
    post_gain,
    pre_gain,
    expert_ids,
    expert_weights,
    w_gate,
    w_up,
    w_down,
):
    rows = query_a.shape[0]
    heads = cum_gates.shape[2]
    width_a = query_a.shape[1] // heads
    width_b = query_b.shape[1] // heads
    group_size = lax.axis_size("sp")
    narrow = lax.axis_size("tp")
    here = lax.axis_index("sp")
    offset = here * rows
    gates_all = lax.all_gather(cum_gates, "sp", axis=0, tiled=True)
    queries_a = query_a.reshape(rows, heads, width_a)
    queries_b = query_b.reshape(rows, heads, width_b)
    blocks = [(queries_a, queries_b, offset + jnp.arange(rows, dtype=jnp.int32), cum_gates)]
    initial = tuple(
        (
            (
                empty_state(block[2].shape[0], heads, width_a),
                empty_state(block[2].shape[0], heads, width_b),
            )
            for block in blocks
        )
    )
    start = jnp.int32(0)
    piece_key_a = lax.all_gather(key_a.reshape(rows, heads, width_a), "sp", axis=0, tiled=True)
    piece_value_a = lax.all_gather(value_a.reshape(rows, heads, width_a), "sp", axis=0, tiled=True)
    piece_key_b = lax.all_gather(key_b.reshape(rows, heads, width_b), "sp", axis=0, tiled=True)
    piece_value_b = lax.all_gather(value_b.reshape(rows, heads, width_b), "sp", axis=0, tiled=True)
    item_count = piece_key_a.shape[0]
    key_pos = jnp.arange(item_count, dtype=jnp.int32)
    updated = []
    for state, (block_a, block_b, position, block_gate) in zip(initial, blocks):

        def compute(current):
            mask = key_pos[None, :] <= position[:, None]
            return (
                update_state(
                    current[0],
                    block_a,
                    piece_key_a,
                    piece_value_a,
                    block_gate[:, 0, :],
                    gates_all[:, 0, :],
                    mask,
                    width_a,
                ),
                update_state(
                    current[1],
                    block_b,
                    piece_key_b,
                    piece_value_b,
                    block_gate[:, 1, :],
                    gates_all[:, 1, :],
                    mask,
                    width_b,
                ),
            )

        updated.append(lax.cond(start <= position[-1], compute, lambda current: current, state))
    folded = tuple(updated)
    attn_a = finish(folded[0][0])
    attn_b = finish(folded[0][1])
    proj = lax.psum_scatter(
        (
            jnp.dot(attn_a, out_a, preferred_element_type=jnp.float32)
            + jnp.dot(attn_b, out_b, preferred_element_type=jnp.float32)
        ).astype(jnp.bfloat16),
        "tp",
        scatter_dimension=0,
        tiled=True,
    )
    post = rms_scale(proj.astype(jnp.float32), post_gain.astype(jnp.float32))
    mid_stream = (residual_in.astype(jnp.float32) + post).astype(jnp.bfloat16)
    normed = rms_scale(mid_stream.astype(jnp.float32), pre_gain.astype(jnp.float32)).astype(
        jnp.bfloat16
    )
    selected_count = expert_ids.shape[1]
    columns = normed.shape[1] // narrow
    slots = rows * selected_count * 5 // (4 * group_size)
    flat_experts = expert_ids.reshape(-1)
    onehot = (flat_experts[:, None] == jnp.arange(group_size, dtype=jnp.int32)[None, :]).astype(
        jnp.int32
    )
    rank = jnp.sum((jnp.cumsum(onehot, axis=0) - onehot) * onehot, axis=1)
    target = flat_experts * slots + rank
    owner = jnp.arange(rows * selected_count, dtype=jnp.int32) // selected_count
    table = jnp.full((group_size * slots,), -1, jnp.int32).at[target].set(owner)
    live = table >= 0
    source = jnp.maximum(table, 0)
    weighting = jnp.sum(
        expert_weights[:, :, None]
        * (
            target.reshape(rows, selected_count)[:, :, None]
            == jnp.arange(group_size * slots, dtype=jnp.int32)[None, None, :]
        ),
        axis=1,
    )
    column_rows = lax.all_to_all(normed, "tp", split_axis=1, concat_axis=0, tiled=True)
    outgoing = jnp.where(live[:, None], column_rows[source], jnp.zeros((), jnp.bfloat16))
    outgoing = outgoing.reshape(group_size, slots, columns)
    arrived = lax.all_to_all(outgoing, "sp", split_axis=0, concat_axis=0, tiled=True)
    flat = arrived.reshape(-1, columns)
    piece = lax.all_gather(flat, "tp", axis=1, tiled=True)
    gate_rows = w_gate[0]
    up_rows = w_up[0]
    gate = jnp.dot(piece, gate_rows, preferred_element_type=jnp.float32)
    upward = jnp.dot(piece, up_rows, preferred_element_type=jnp.float32)
    hidden_rows = (jax.nn.silu(gate) * upward).astype(jnp.bfloat16)
    hidden = hidden_rows.reshape(arrived.shape[0], arrived.shape[1], -1)
    flat_hidden = hidden.reshape(-1, hidden.shape[2])
    down_cols = w_down[0]
    summed = lax.psum_scatter(
        lax.dot_general(
            down_cols, flat_hidden, (((0,), (1,)), ((), ())), preferred_element_type=jnp.float32
        ).astype(jnp.bfloat16),
        "tp",
        scatter_dimension=0,
        tiled=True,
    )
    returned = lax.all_to_all(
        summed.reshape(columns, group_size, slots), "sp", split_axis=1, concat_axis=1, tiled=True
    )
    mixture_cols = jnp.einsum(
        "te,ce->tc",
        weighting,
        returned.reshape(columns, group_size * slots).astype(jnp.float32),
        precision=lax.Precision.HIGHEST,
    )
    mixture = lax.all_to_all(
        mixture_cols.astype(jnp.bfloat16), "tp", split_axis=0, concat_axis=1, tiled=True
    ).astype(mixture_cols.dtype)
    return (mid_stream.astype(jnp.float32) + mixture).astype(jnp.bfloat16)


def solution(mesh):
    placed = (
        P(("sp", "tp"), None),
        P("sp", "tp"),
        P("sp", "tp"),
        P("sp", "tp"),
        P("sp", "tp"),
        P("sp", "tp"),
        P("sp", "tp"),
        P("sp", None, "tp"),
        P("tp", None),
        P("tp", None),
        P(),
        P(),
        P("sp", None),
        P("sp", None),
        P("sp", None, "tp"),
        P("sp", None, "tp"),
        P("sp", "tp", None),
    )
    return jax.shard_map(
        per_device, mesh=mesh, in_specs=placed, out_specs=P(("sp", "tp"), None), check_vma=False
    )
```

profile of v0, /device:TPU:0, one launch (start us, length us, event | category | flops | bytes accessed | tf_op | source)
XLA Modules:
  0.0 352.2 jit_solution(581141033529459929)
XLA Ops:
  6.5 1.8 copy.59
  8.4 1.7 copy.60
  10.2 1.8 copy.61
  12.0 1.8 copy.62
  13.9 0.6 slice.21
  15.0 16.0 %all_gather.19 = f32[2048,2,4]{0,2,1:T(4,128)S(1)} all-gather(f32[256,2,4]{0,2,1:T(4,128)} %param.26), channel_id=1, replica_groups=mesh['sp'=8,'tp'=4] {'sp'}, dimensions={0}, use_global_device_ids=true | all-gather | bytes 73728 | tf_op jit(solution)/shard_map/all_gather | solution.py:71
  31.0 4.8 %all-gather.6.cloned.1.call-done = bf16[2048,4,64]{0,2,1:T(8,128)(2,1)} async-done(((bf16[256,4,64]{0,2,1:T(8,128)(2,1)}), bf16[2048,4,64]{0,2,1:T(8,128)(2,1)}) %all-gather.6.cloned.1.call-update) | async-done | bytes 1048592 | tf_op jit(solution)/shard_map/all_gather | solution.py:85
  35.9 25.3 %all-gather.8.cloned.1.call-done = bf16[2048,4,64]{0,2,1:T(8,128)(2,1)} async-done(((bf16[256,4,64]{0,2,1:T(8,128)(2,1)}), bf16[2048,4,64]{0,2,1:T(8,128)(2,1)}) %all-gather.8.cloned.1.call-update) | async-done | bytes 1048592 | tf_op jit(solution)/shard_map/all_gather | solution.py:86
  61.2 31.0 %all-gather.10.cloned.1.call-done = bf16[2048,4,128]{0,2,1:T(8,128)(2,1)} async-done(((bf16[256,4,128]{0,2,1:T(8,128)(2,1)}), bf16[2048,4,128]{0,2,1:T(8,128)(2,1)}) %all-gather.10.cloned.1.call-update) | async-done | bytes 2097168 | tf_op jit(solution)/shard_map/all_gather | solution.py:87
  92.2 31.1 %all-gather.12.cloned.1.call-done = bf16[2048,4,128]{0,2,1:T(8,128)(2,1)} async-done(((bf16[256,4,128]{0,2,1:T(8,128)(2,1)}), bf16[2048,4,128]{0,2,1:T(8,128)(2,1)}) %all-gather.12.cloned.1.call-update) | async-done | bytes 2097168 | tf_op jit(solution)/shard_map/all_gather | solution.py:88
  123.3 22.6 %conditional.1 = (f32[4,256]{1,0:T(4,128)S(1)}, f32[4,256,64]{1,2,0:T(8,128)S(1)}, f32[4,256]{1,0:T(4,128)S(1)}, f32[4,256,128]{1,2,0:T(8,128)S(1)}) conditional(s32[]{:T(128)} %bitcast.9, () %tuple.13, (s32[2048]{0:T(1024)S(1)}, s32[256]{0:T(256)S(1)}, bf16[256,256]{1,0:T(8,128)(2,1)}, bf16[2048,4,64]{0,2,1:T(8,128)(2,1)}, f32[256,2,4]{0,2,1:T(4,128)}, ...), branch_computations={%region_0.0_spmd, %region_1.6_spmd} | conditional | flops 1682438144 | bytes 83133552 | solution.py:119
  123.3 0.7 slice_bitcast_fusion.3
  124.0 1.0 copy.63
  125.1 0.4 broadcast_compare_fusion
  125.4 2.7 fusion.53
  128.2 4.5 %select_reduce_fusion = (f32[4,256]{1,0:T(4,128)S(1)}, f32[4,256]{1,0:T(4,128)S(1)}, f32[4,256,2048]{2,1,0:T(8,128)S(1)}) fusion(f32[4,2048]{1,0:T(4,128)S(1)} %get-tuple-element.97, f32[4,256]{1,0:T(4,128)S(1)} %get-tuple-element.99, pred[256,2048]{1,0:T(8,128)(4,1)S(1)} %broadcast_compare_fusion, f32[4,2048]{1,0:T(4,128)S(1)} %get-tuple-element.96, ...), kind=kOutput, calls=%fused_computation.3 | convolution fusion | flops 557840384 | bytes 19742720 | tf_op jit(solution)/shard_map/cond/branch_1_fun/rhd,khd->hrk/dot_general | solution.py:24
  132.7 2.8 fusion.6
  135.5 5.9 %fusion.3 = (f32[4,256]{1,0:T(4,128)S(1)}, f32[4,256]{1,0:T(4,128)S(1)}) fusion(f32[4,256,2048]{2,1,0:T(8,128)S(1)} %get-tuple-element.100, f32[4,256]{1,0:T(4,128)S(1)} %get-tuple-element.101, f32[4,2048]{1,0:T(4,128)S(1)} %get-tuple-element.97, f32[4,256]{1,0:T(4,128)S(1)} %get-tuple-element.99, pred[256,2048]{1,0:T(8,128)(4,1)S(1)} %broadcast_compare_fusion, ...), kind=kLoop, calls=%fused_computation.11 | loop fusion | flops 25163776 | bytes 17391616 | tf_op jit(solution)/shard_map/cond/branch_1_fun/reduce_sum | solution.py:30
  141.4 4.3 %fusion.4 = f32[4,256,128]{1,2,0:T(8,128)S(1)} fusion(bf16[2048,4,128]{0,2,1:T(8,128)(2,1)} %get-tuple-element.88, f32[4,256,2048]{2,1,0:T(8,128)S(1)} %get-tuple-element.100, f32[4,256]{1,0:T(4,128)S(1)} %get-tuple-element.101, f32[4,2048]{1,0:T(4,128)S(1)} %get-tuple-element.97, f32[4,256]{1,0:T(4,128)S(1)} %get-tuple-element.99, ...), kind=kOutput, calls=%fused_computation.12 | convolution fusion | flops 549453824 | bytes 11575296 | tf_op jit(solution)/shard_map/cond | solution.py:119
  146.0 1.7 fusion.54
  147.8 1.7 fusion.29
  149.7 0.1 eq.42
  149.8 0.1 eq.38
  150.0 1.1 reduce-window.6
  151.1 0.2 slice_reduce_fusion
  151.5 0.1 reduce_sum.60
  151.7 0.1 mul.94
  151.8 2.4 scatter_custom_fusion
  154.3 22.3 %reduce-scatter.3.cloned.1.call-done = bf16[64,2048]{1,0:T(8,128)(2,1)} async-done(((bf16[256,2048]{1,0:T(8,128)(2,1)}), bf16[64,2048]{1,0:T(8,128)(2,1)}) %reduce-scatter.3.cloned.1.call-update) | async-done | bytes 262160 | tf_op jit(solution)/shard_map/reduce_scatter | solution.py:123
  176.6 1.1 fusion.34
  177.8 1.3 fusion.38
  179.0 0.7 copy-done.1
  179.9 0.7 copy.87
  180.6 3.4 all-to-all-start
  184.2 5.3 %all-to-all-done = bf16[64,4,512]{2,0,1:T(8,128)(2,1)S(1)} async-done(((bf16[64,4,512]{2,0,1:T(8,128)(2,1)}), bf16[64,4,512]{2,0,1:T(8,128)(2,1)S(1)}, u32[]{:S(2)}, u32[]{:S(2)}) %all-to-all-start) | async-done | bytes 262176 | tf_op jit(solution)/shard_map/all_to_all | solution.py:158
  189.5 2.8 gather_fusion
  192.2 0.2 broadcast_select_fusion
  192.4 22.6 %all_to_all.42 = bf16[8,80,512]{2,1,0:T(8,128)(2,1)} all-to-all(bf16[8,80,512]{2,1,0:T(8,128)(2,1)S(1)} %broadcast_select_fusion), channel_id=1, replica_groups=mesh['sp'=8,'tp'=4] {'sp'}, dimensions={0} | all-to-all | bytes 1310720 | tf_op jit(solution)/shard_map/all_to_all | solution.py:161
  215.1 37.2 %all-gather.14.cloned.1.call-done = bf16[640,2048]{1,0:T(8,128)(2,1)} async-done(((bf16[640,512]{1,0:T(8,128)(2,1)}), bf16[640,2048]{1,0:T(8,128)(2,1)}) %all-gather.14.cloned.1.call-update) | async-done | bytes 2621456 | tf_op jit(solution)/shard_map/all_gather | solution.py:163
  252.4 7.4 %fusion.19 = f32[640,1024]{1,0:T(8,128)} fusion(bf16[640,2048]{1,0:T(8,128)(2,1)} %all-gather.14.cloned.1.call-done, bf16[1,2048,1024]{2,1,0:T(8,128)(2,1)} %param.34), kind=kOutput, calls=%fused_computation.32 | convolution fusion | flops 2684354560 | bytes 9437184 | tf_op jit(solution)/shard_map/dot_general | solution.py:167
  259.7 12.3 %fusion.26 = bf16[2048,640]{0,1:T(8,128)(2,1)} fusion(bf16[1,1024,2048]{2,1,0:T(8,128)(2,1)} %param.35, f32[640,1024]{1,0:T(8,128)} %fusion.19, bf16[640,2048]{1,0:T(8,128)(2,1)} %all-gather.14.cloned.1.call-done, bf16[1,2048,1024]{2,1,0:T(8,128)(2,1)} %param.33), kind=kOutput, calls=%fused_computation.37 | convolution fusion | flops 5373952000 | bytes 16252928 | tf_op jit(solution)/shard_map/dot_general | solution.py:173
  272.0 39.7 %reduce-scatter.5.cloned.1.call-done = bf16[512,640]{0,1:T(8,128)(2,1)} async-done(((bf16[2048,640]{0,1:T(8,128)(2,1)}), bf16[512,640]{0,1:T(8,128)(2,1)}) %reduce-scatter.5.cloned.1.call-update) | async-done | bytes 655376 | tf_op jit(solution)/shard_map/reduce_scatter | solution.py:172
  311.8 4.6 %all-to-all-start.2 = ((bf16[512,8,80]{0,2,1:T(8,128)(2,1)}), bf16[512,8,80]{0,2,1:T(8,128)(2,1)S(1)}, u32[]{:S(2)}, u32[]{:S(2)}) async-start(bf16[512,8,80]{0,2,1:T(8,128)(2,1)} %bitcast.106), calls=%async_computation.4 | async-start | bytes 1310720 | tf_op jit(solution)/shard_map/all_to_all | solution.py:180
  316.4 0.2 select_reduce_fusion.2
  316.7 17.8 %all-to-all-done.2 = bf16[512,8,80]{0,2,1:T(8,128)(2,1)S(1)} async-done(((bf16[512,8,80]{0,2,1:T(8,128)(2,1)}), bf16[512,8,80]{0,2,1:T(8,128)(2,1)S(1)}, u32[]{:S(2)}, u32[]{:S(2)}) %all-to-all-start.2) | async-done | bytes 655392 | tf_op jit(solution)/shard_map/all_to_all | solution.py:180
  334.5 0.8 convolution_convert_fusion
  335.3 8.3 %all_to_all.43 = bf16[4,64,512]{2,1,0:T(8,128)(2,1)S(1)} all-to-all(bf16[4,64,512]{2,1,0:T(8,128)(2,1)S(1)} %bitcast.104), channel_id=1, replica_groups=mesh['sp'=8,'tp'=4] {'tp'}, dimensions={0} | all-to-all | bytes 524288 | tf_op jit(solution)/shard_map/all_to_all | solution.py:189
  343.7 1.7 fusion.41
  (59 shorter events, 1.2 us)
Async XLA Ops:
  6.5 141.2 %copy-start = (bf16[512,2048]{1,0:T(8,128)(2,1)S(1)}, bf16[512,2048]{1,0:T(8,128)(2,1)}, u32[]{:S(2)}) copy-start(bf16[512,2048]{1,0:T(8,128)(2,1)} %param.28) | copy-start | bytes 6291460
  6.5 29.3 %all-gather.6.cloned.1.call-start = ((), (), s32[]{:S(2)}) async-start(), calls=%async_computation.6 | async-start | bytes 1179648 | tf_op jit(solution)/shard_map/all_gather | solution.py:85
  8.4 52.8 %all-gather.8.cloned.1.call-start = ((), (), s32[]{:S(2)}) async-start(), calls=%async_computation.7 | async-start | bytes 1179648 | tf_op jit(solution)/shard_map/all_gather | solution.py:86
  10.1 82.1 %all-gather.10.cloned.1.call-start = ((), (), s32[]{:S(2)}) async-start(), calls=%async_computation.8 | async-start | bytes 2359296 | tf_op jit(solution)/shard_map/all_gather | solution.py:87
  12.0 111.3 %all-gather.12.cloned.1.call-start = ((), (), s32[]{:S(2)}) async-start(), calls=%async_computation.9 | async-start | bytes 2359296 | tf_op jit(solution)/shard_map/all_gather | solution.py:88
  13.8 162.8 %reduce-scatter.3.cloned.1.call-start = ((), (), s32[]{:S(2)}) async-start(), calls=%async_computation.10 | async-start | bytes 1310720 | tf_op jit(solution)/shard_map/reduce_scatter | solution.py:123
  124.0 4.1 %copy-start.9 = (bf16[256,512]{1,0:T(8,128)(2,1)S(1)}, bf16[256,512]{1,0:T(8,128)(2,1)}, u32[]{:S(2)}) copy-start(bf16[256,512]{1,0:T(8,128)(2,1)} %get-tuple-element.48) | copy-start | bytes 786436 | tf_op jit(solution)/shard_map/cond
  125.1 3.1 copy-start.7
  128.2 4.5 %copy-start.8 = (bf16[2048,4,64]{0,2,1:T(8,128)(2,1)S(1)}, bf16[2048,4,64]{0,2,1:T(8,128)(2,1)}, u32[]{:S(2)}) copy-start(bf16[2048,4,64]{0,2,1:T(8,128)(2,1)} %get-tuple-element.33) | copy-start | bytes 3145732 | tf_op jit(solution)/shard_map/cond
  145.9 3.6 %copy-start.5 = (s32[256,2]{0,1:T(2,128)S(1)}, s32[256,2]{0,1:T(2,128)}, u32[]{:S(2)}) copy-start(s32[256,2]{0,1:T(2,128)} %param.31) | copy-start | bytes 6148
  146.0 4.0 %copy-start.3 = (bf16[2048]{0:T(1024)(128)(2,1)S(1)}, bf16[2048]{0:T(1024)(128)(2,1)}, u32[]{:S(2)}) copy-start(bf16[2048]{0:T(1024)(128)(2,1)} %param.29) | copy-start | bytes 12292
  146.0 4.0 %copy-start.4 = (bf16[2048]{0:T(1024)(128)(2,1)S(1)}, bf16[2048]{0:T(1024)(128)(2,1)}, u32[]{:S(2)}) copy-start(bf16[2048]{0:T(1024)(128)(2,1)} %param.30) | copy-start | bytes 12292
  146.0 31.7 %copy-start.2 = (bf16[64,2048]{1,0:T(8,128)(2,1)S(1)}, bf16[64,2048]{1,0:T(8,128)(2,1)}, u32[]{:S(2)}) copy-start(bf16[64,2048]{1,0:T(8,128)(2,1)} %param.19) | copy-start | bytes 786436
  179.0 0.7 copy-start.1
  180.6 8.9 %all-to-all-start = ((bf16[64,4,512]{2,0,1:T(8,128)(2,1)}), bf16[64,4,512]{2,0,1:T(8,128)(2,1)S(1)}, u32[]{:S(2)}, u32[]{:S(2)}) async-start(bf16[64,4,512]{2,0,1:T(8,128)(2,1)} %bitcast.94), calls=%async_computation.1 | async-start | bytes 524288 | tf_op jit(solution)/shard_map/all_to_all | solution.py:158
  184.0 68.3 %all-gather.14.cloned.1.call-start = ((), (), s32[]{:S(2)}) async-start(), calls=%async_computation.11 | async-start | bytes 3276800 | tf_op jit(solution)/shard_map/all_gather | solution.py:163
  215.1 96.7 %reduce-scatter.5.cloned.1.call-start = ((), (), s32[]{:S(2)}) async-start(), calls=%async_computation.12 | async-start | bytes 3276800 | tf_op jit(solution)/shard_map/reduce_scatter | solution.py:172
  259.7 56.7 %copy-start.6 = (f32[256,2]{0,1:T(2,128)S(1)}, f32[256,2]{0,1:T(2,128)}, u32[]{:S(2)}) copy-start(f32[256,2]{0,1:T(2,128)} %param.32) | copy-start | bytes 6148
  311.8 22.7 %all-to-all-start.2 = ((bf16[512,8,80]{0,2,1:T(8,128)(2,1)}), bf16[512,8,80]{0,2,1:T(8,128)(2,1)S(1)}, u32[]{:S(2)}, u32[]{:S(2)}) async-start(bf16[512,8,80]{0,2,1:T(8,128)(2,1)} %bitcast.106), calls=%async_computation.4 | async-start | bytes 1310720 | tf_op jit(solution)/shard_map/all_to_all | solution.py:180
Sparse Core Ops, SparseCore 0:
  8.9 26.9 all-gather.5
  37.5 23.6 all-gather.7
  62.8 29.3 all-gather.9
  93.6 29.6 all-gather.11
  149.6 26.9 reduce-scatter.2
  215.2 37.1 all-gather.13
  272.2 39.5 reduce-scatter.4
where the time goes:
time: 353 us; the launch traced here: 352 us
  waiting for transfers between devices  215 us (61%)
  blocking collectives  46.9 us (13%)
  matrix products  38.2 us (11%)
  local copies, waits for them, and re-layouts  17.2 us (5%)
  between operations  14.4 us (4%)
  other arithmetic  12.3 us (3%)
  starting transfers between devices  8.24 us (2%)
    reduce_scatter x1, waiting for transfers between devices, per_device(): lax.psum_scatter(lax.dot_general(down_cols, flat_hidden, (((0,), (1,)), (...  39.7 us
    all_gather x1, waiting for transfers between devices, per_device(): piece = lax.all_gather(flat, 'tp', axis=1, tiled=True)  37.2 us
    all_gather x1, waiting for transfers between devices, per_device(): lax.all_gather(value_b.reshape(rows, heads, width_b), 'sp', axis=0, tiled...  31.1 us
    all_gather x1, waiting for transfers between devices, per_device(): lax.all_gather(key_b.reshape(rows, heads, width_b), 'sp', axis=0, tiled=T...  31 us
    all_gather x1, waiting for transfers between devices, per_device(): lax.all_gather(value_a.reshape(rows, heads, width_a), 'sp', axis=0, tiled...  25.3 us
    all_to_all x1, blocking collectives, per_device(): lax.all_to_all(outgoing, 'sp', split_axis=0, concat_axis=0, tiled=True)  22.6 us
    reduce_scatter x1, waiting for transfers between devices, per_device(): lax.psum_scatter((jnp.dot(attn_a, out_a, preferred_element_type=jnp.float...  22.3 us
    all_to_all x1, waiting for transfers between devices, per_device(): lax.all_to_all(summed.reshape(columns, group_size, slots), 'sp', split_ax...  17.8 us
  transfers between devices with their start and end apart: 9, of which 9 were waited for; matrix products, arithmetic and copies ran while one was open for 3% of the time, Pallas kernels for 0%

commit v1 on v0

--- a/solution.py
+++ b/solution.py
@@ -2,6 +2,7 @@
 import jax.numpy as jnp
 from jax import lax
 from jax.sharding import PartitionSpec as P
+from jax.lax import all_gather
 
 eps_norm = 1e-06
 big_neg = -1e30
@@ -160,7 +161,7 @@
     outgoing = outgoing.reshape(group_size, slots, columns)
     arrived = lax.all_to_all(outgoing, "sp", split_axis=0, concat_axis=0, tiled=True)
     flat = arrived.reshape(-1, columns)
-    piece = lax.all_gather(flat, "tp", axis=1, tiled=True)
+    piece = jnp.concatenate(all_gather(flat, "tp"), 1)
     gate_rows = w_gate[0]
     up_rows = w_up[0]
     gate = jnp.dot(piece, gate_rows, preferred_element_type=jnp.float32)

time: 353 us -> 351 us (level)
  matrix products: 38.2 us -> 31.8 us
  local copies, waits for them, and re-layouts: 17.2 us -> 21.6 us
    dot_general x1, matrix products: 12.3 us -> 4.18 us  [per_device(): lax.dot_general(down_cols, flat_hidden, (((0,), (1,)), ((), ())), preferr...]
    all_gather x0 -> x1, local copies, waits for them, and re-layouts: none -> 4.38 us  [per_device(): piece = jnp.concatenate(all_gather(flat, 'tp'), 1)]
    unnamed x19 -> x25, local copies, waits for them, and re-layouts: 7.91 us -> 7.93 us
where the time goes in v1:
time: 351 us; the launch traced here: 350 us
  waiting for transfers between devices  215 us (61%)
  blocking collectives  46.9 us (13%)
  matrix products  31.8 us (9%)
  local copies, waits for them, and re-layouts  21.6 us (6%)
  between operations  14.5 us (4%)
  other arithmetic  12.3 us (4%)
  starting transfers between devices  8.27 us (2%)
    reduce_scatter x1, waiting for transfers between devices, per_device(): lax.psum_scatter(lax.dot_general(down_cols, flat_hidden, (((0,), (1,)), (...  39.7 us
    all_gather x1, waiting for transfers between devices, per_device(): piece = jnp.concatenate(all_gather(flat, 'tp'), 1)  37.4 us
    all_gather x1, waiting for transfers between devices, per_device(): lax.all_gather(value_b.reshape(rows, heads, width_b), 'sp', axis=0, tiled...  31.1 us
    all_gather x1, waiting for transfers between devices, per_device(): lax.all_gather(key_b.reshape(rows, heads, width_b), 'sp', axis=0, tiled=T...  31 us
    all_gather x1, waiting for transfers between devices, per_device(): lax.all_gather(value_a.reshape(rows, heads, width_a), 'sp', axis=0, tiled...  25.1 us
    all_to_all x1, blocking collectives, per_device(): lax.all_to_all(outgoing, 'sp', split_axis=0, concat_axis=0, tiled=True)  22.7 us
    reduce_scatter x1, waiting for transfers between devices, per_device(): lax.psum_scatter((jnp.dot(attn_a, out_a, preferred_element_type=jnp.float...  22.3 us
    all_to_all x1, waiting for transfers between devices, per_device(): lax.all_to_all(summed.reshape(columns, group_size, slots), 'sp', split_ax...  17.8 us
  transfers between devices with their start and end apart: 9, of which 9 were waited for; matrix products, arithmetic and copies ran while one was open for 3% of the time, Pallas kernels for 0%

profile of v1, /device:TPU:0, one launch (start us, length us, event | category | flops | bytes accessed | tf_op | source)
XLA Modules:
  0.0 350.4 jit_solution(4038256579388415200)
XLA Ops:
  6.5 1.8 copy.77
  8.4 1.7 copy.78
  10.2 1.8 copy.79
  12.0 1.8 copy.80
  13.9 0.6 slice.21
  15.2 16.0 %all_gather.19 = f32[2048,2,4]{0,2,1:T(4,128)S(1)} all-gather(f32[256,2,4]{0,2,1:T(4,128)} %param.26), channel_id=1, replica_groups=mesh['sp'=8,'tp'=4] {'sp'}, dimensions={0}, use_global_device_ids=true | all-gather | bytes 73728 | tf_op jit(solution)/shard_map/all_gather | solution.py:72
  31.1 4.8 %all-gather.6.cloned.1.call-done = bf16[2048,4,64]{0,2,1:T(8,128)(2,1)} async-done(((bf16[256,4,64]{0,2,1:T(8,128)(2,1)}), bf16[2048,4,64]{0,2,1:T(8,128)(2,1)}) %all-gather.6.cloned.1.call-update) | async-done | bytes 1048592 | tf_op jit(solution)/shard_map/all_gather | solution.py:86
  36.0 25.1 %all-gather.8.cloned.1.call-done = bf16[2048,4,64]{0,2,1:T(8,128)(2,1)} async-done(((bf16[256,4,64]{0,2,1:T(8,128)(2,1)}), bf16[2048,4,64]{0,2,1:T(8,128)(2,1)}) %all-gather.8.cloned.1.call-update) | async-done | bytes 1048592 | tf_op jit(solution)/shard_map/all_gather | solution.py:87
  61.1 31.0 %all-gather.10.cloned.1.call-done = bf16[2048,4,128]{0,2,1:T(8,128)(2,1)} async-done(((bf16[256,4,128]{0,2,1:T(8,128)(2,1)}), bf16[2048,4,128]{0,2,1:T(8,128)(2,1)}) %all-gather.10.cloned.1.call-update) | async-done | bytes 2097168 | tf_op jit(solution)/shard_map/all_gather | solution.py:88
  92.1 31.1 %all-gather.12.cloned.1.call-done = bf16[2048,4,128]{0,2,1:T(8,128)(2,1)} async-done(((bf16[256,4,128]{0,2,1:T(8,128)(2,1)}), bf16[2048,4,128]{0,2,1:T(8,128)(2,1)}) %all-gather.12.cloned.1.call-update) | async-done | bytes 2097168 | tf_op jit(solution)/shard_map/all_gather | solution.py:89
  123.2 22.6 %conditional.1 = (f32[4,256]{1,0:T(4,128)S(1)}, f32[4,256,64]{1,2,0:T(8,128)S(1)}, f32[4,256]{1,0:T(4,128)S(1)}, f32[4,256,128]{1,2,0:T(8,128)S(1)}) conditional(s32[]{:T(128)} %bitcast.9, () %tuple.13, (s32[2048]{0:T(1024)S(1)}, s32[256]{0:T(256)S(1)}, bf16[256,256]{1,0:T(8,128)(2,1)}, bf16[2048,4,64]{0,2,1:T(8,128)(2,1)}, f32[256,2,4]{0,2,1:T(4,128)}, ...), branch_computations={%region_0.0_spmd, %region_1.6_spmd} | conditional | flops 1682438144 | bytes 83133552 | solution.py:120
  123.2 0.7 slice_bitcast_fusion.3
  123.9 1.0 copy.81
  125.0 0.4 broadcast_compare_fusion
  125.4 2.7 fusion.50
  128.1 4.5 %select_reduce_fusion = (f32[4,256]{1,0:T(4,128)S(1)}, f32[4,256]{1,0:T(4,128)S(1)}, f32[4,256,2048]{2,1,0:T(8,128)S(1)}) fusion(f32[4,2048]{1,0:T(4,128)S(1)} %get-tuple-element.107, f32[4,256]{1,0:T(4,128)S(1)} %get-tuple-element.109, pred[256,2048]{1,0:T(8,128)(4,1)S(1)} %broadcast_compare_fusion, f32[4,2048]{1,0:T(4,128)S(1)} %get-tuple-element.106, ...), kind=kOutput, calls=%fused_computation.3 | convolution fusion | flops 557840384 | bytes 19742720 | tf_op jit(solution)/shard_map/cond/branch_1_fun/rhd,khd->hrk/dot_general | solution.py:25
  132.6 2.8 fusion.6
  135.4 5.9 %fusion.3 = (f32[4,256]{1,0:T(4,128)S(1)}, f32[4,256]{1,0:T(4,128)S(1)}) fusion(f32[4,256,2048]{2,1,0:T(8,128)S(1)} %get-tuple-element.110, f32[4,256]{1,0:T(4,128)S(1)} %get-tuple-element.111, f32[4,2048]{1,0:T(4,128)S(1)} %get-tuple-element.107, f32[4,256]{1,0:T(4,128)S(1)} %get-tuple-element.109, pred[256,2048]{1,0:T(8,128)(4,1)S(1)} %broadcast_compare_fusion, ...), kind=kLoop, calls=%fused_computation.11 | loop fusion | flops 25163776 | bytes 17391616 | tf_op jit(solution)/shard_map/cond/branch_1_fun/reduce_sum | solution.py:31
  141.3 4.3 %fusion.4 = f32[4,256,128]{1,2,0:T(8,128)S(1)} fusion(bf16[2048,4,128]{0,2,1:T(8,128)(2,1)} %get-tuple-element.98, f32[4,256,2048]{2,1,0:T(8,128)S(1)} %get-tuple-element.110, f32[4,256]{1,0:T(4,128)S(1)} %get-tuple-element.111, f32[4,2048]{1,0:T(4,128)S(1)} %get-tuple-element.107, f32[4,256]{1,0:T(4,128)S(1)} %get-tuple-element.109, ...), kind=kOutput, calls=%fused_computation.12 | convolution fusion | flops 549453824 | bytes 11575296 | tf_op jit(solution)/shard_map/cond | solution.py:120
  145.9 1.7 fusion.51
  147.7 1.7 fusion.29
  149.6 0.1 eq.42
  149.9 1.1 reduce-window.6
  151.1 0.2 slice_reduce_fusion
  151.4 0.1 reduce_sum.60
  151.8 2.4 scatter_custom_fusion
  154.2 22.3 %reduce-scatter.3.cloned.1.call-done = bf16[64,2048]{1,0:T(8,128)(2,1)} async-done(((bf16[256,2048]{1,0:T(8,128)(2,1)}), bf16[64,2048]{1,0:T(8,128)(2,1)}) %reduce-scatter.3.cloned.1.call-update) | async-done | bytes 262160 | tf_op jit(solution)/shard_map/reduce_scatter | solution.py:124
  176.6 1.1 fusion.32
  177.7 1.3 fusion.36
  179.0 0.7 copy-done.2
  179.8 0.7 copy.106
  180.5 3.4 all-to-all-start
  184.1 5.3 %all-to-all-done = bf16[64,4,512]{2,0,1:T(8,128)(2,1)S(1)} async-done(((bf16[64,4,512]{2,0,1:T(8,128)(2,1)}), bf16[64,4,512]{2,0,1:T(8,128)(2,1)S(1)}, u32[]{:S(2)}, u32[]{:S(2)}) %all-to-all-start) | async-done | bytes 262176 | tf_op jit(solution)/shard_map/all_to_all | solution.py:159
  189.4 2.8 gather_fusion
  192.2 0.2 broadcast_select_fusion
  192.3 22.7 %all_to_all.42 = bf16[8,80,512]{2,1,0:T(8,128)(2,1)} all-to-all(bf16[8,80,512]{2,1,0:T(8,128)(2,1)S(1)} %broadcast_select_fusion), channel_id=1, replica_groups=mesh['sp'=8,'tp'=4] {'sp'}, dimensions={0} | all-to-all | bytes 1310720 | tf_op jit(solution)/shard_map/all_to_all | solution.py:162
  215.0 37.4 %all-gather.14.cloned.1.call-done = bf16[4,640,512]{2,1,0:T(8,128)(2,1)} async-done(((bf16[1,640,512]{2,1,0:T(8,128)(2,1)}), bf16[4,640,512]{2,1,0:T(8,128)(2,1)}) %all-gather.14.cloned.1.call-update) | async-done | bytes 2621456 | tf_op jit(solution)/shard_map/all_gather | solution.py:164
  252.4 4.4 %copy.90 = bf16[4,640,512]{1,2,0:T(8,128)(2,1)} copy(bf16[4,640,512]{2,1,0:T(8,128)(2,1)} %all-gather.14.cloned.1.call-done) | data formatting | bytes 5242880 | tf_op jit(solution)/shard_map/all_gather | solution.py:164
  256.8 5.6 %fusion.19 = f32[640,1024]{1,0:T(8,128)S(1)} fusion(bf16[640,2048]{0,1:T(8,128)(2,1)} %bitcast.99, bf16[1,2048,1024]{2,1,0:T(8,128)(2,1)} %param.34), kind=kOutput, calls=%fused_computation.32 | convolution fusion | flops 2684354560 | bytes 9437184 | tf_op jit(solution)/shard_map/dot_general | solution.py:168
  262.5 3.5 multiply_convert_fusion
  266.0 4.2 %fusion.26 = bf16[2048,640]{0,1:T(8,128)(2,1)} fusion(bf16[640,1024]{1,0:T(8,128)(2,1)S(1)} %multiply_convert_fusion, bf16[1,1024,2048]{2,1,0:T(8,128)(2,1)S(1)} %copy-done.9), kind=kOutput, calls=%fused_computation.37 | convolution fusion | flops 2685665280 | bytes 8126464 | tf_op jit(solution)/shard_map/dot_general | solution.py:174
  270.2 39.7 %reduce-scatter.5.cloned.1.call-done = bf16[512,640]{0,1:T(8,128)(2,1)} async-done(((bf16[2048,640]{0,1:T(8,128)(2,1)}), bf16[512,640]{0,1:T(8,128)(2,1)}) %reduce-scatter.5.cloned.1.call-update) | async-done | bytes 655376 | tf_op jit(solution)/shard_map/reduce_scatter | solution.py:173
  309.9 4.6 %all-to-all-start.2 = ((bf16[512,8,80]{0,2,1:T(8,128)(2,1)}), bf16[512,8,80]{0,2,1:T(8,128)(2,1)S(1)}, u32[]{:S(2)}, u32[]{:S(2)}) async-start(bf16[512,8,80]{0,2,1:T(8,128)(2,1)} %bitcast.110), calls=%async_computation.4 | async-start | bytes 1310720 | tf_op jit(solution)/shard_map/all_to_all | solution.py:181
  314.6 0.2 select_reduce_fusion.2
  314.8 17.8 %all-to-all-done.2 = bf16[512,8,80]{0,2,1:T(8,128)(2,1)S(1)} async-done(((bf16[512,8,80]{0,2,1:T(8,128)(2,1)}), bf16[512,8,80]{0,2,1:T(8,128)(2,1)S(1)}, u32[]{:S(2)}, u32[]{:S(2)}) %all-to-all-start.2) | async-done | bytes 655392 | tf_op jit(solution)/shard_map/all_to_all | solution.py:181
  332.7 0.8 convolution_convert_fusion
  333.5 8.3 %all_to_all.43 = bf16[4,64,512]{2,1,0:T(8,128)(2,1)S(1)} all-to-all(bf16[4,64,512]{2,1,0:T(8,128)(2,1)S(1)} %bitcast.108), channel_id=1, replica_groups=mesh['sp'=8,'tp'=4] {'tp'}, dimensions={0} | all-to-all | bytes 524288 | tf_op jit(solution)/shard_map/all_to_all | solution.py:190
  341.8 1.7 fusion.39
  (67 shorter events, 1.5 us)
Async XLA Ops:
  6.5 141.1 %copy-start = (bf16[512,2048]{1,0:T(8,128)(2,1)S(1)}, bf16[512,2048]{1,0:T(8,128)(2,1)}, u32[]{:S(2)}) copy-start(bf16[512,2048]{1,0:T(8,128)(2,1)} %param.28) | copy-start | bytes 6291460
  6.5 29.4 %all-gather.6.cloned.1.call-start = ((), (), s32[]{:S(2)}) async-start(), calls=%async_computation.6 | async-start | bytes 1179648 | tf_op jit(solution)/shard_map/all_gather | solution.py:86
  8.4 52.8 %all-gather.8.cloned.1.call-start = ((), (), s32[]{:S(2)}) async-start(), calls=%async_computation.7 | async-start | bytes 1179648 | tf_op jit(solution)/shard_map/all_gather | solution.py:87
  10.1 82.0 %all-gather.10.cloned.1.call-start = ((), (), s32[]{:S(2)}) async-start(), calls=%async_computation.8 | async-start | bytes 2359296 | tf_op jit(solution)/shard_map/all_gather | solution.py:88
  12.0 111.2 %all-gather.12.cloned.1.call-start = ((), (), s32[]{:S(2)}) async-start(), calls=%async_computation.9 | async-start | bytes 2359296 | tf_op jit(solution)/shard_map/all_gather | solution.py:89
  13.8 162.7 %reduce-scatter.3.cloned.1.call-start = ((), (), s32[]{:S(2)}) async-start(), calls=%async_computation.10 | async-start | bytes 1310720 | tf_op jit(solution)/shard_map/reduce_scatter | solution.py:124
  123.9 4.1 %copy-start.12 = (bf16[256,512]{1,0:T(8,128)(2,1)S(1)}, bf16[256,512]{1,0:T(8,128)(2,1)}, u32[]{:S(2)}) copy-start(bf16[256,512]{1,0:T(8,128)(2,1)} %get-tuple-element.48) | copy-start | bytes 786436 | tf_op jit(solution)/shard_map/cond
  125.0 3.1 copy-start.10
  128.1 4.5 %copy-start.11 = (bf16[2048,4,64]{0,2,1:T(8,128)(2,1)S(1)}, bf16[2048,4,64]{0,2,1:T(8,128)(2,1)}, u32[]{:S(2)}) copy-start(bf16[2048,4,64]{0,2,1:T(8,128)(2,1)} %get-tuple-element.33) | copy-start | bytes 3145732 | tf_op jit(solution)/shard_map/cond
  145.8 3.6 %copy-start.6 = (s32[256,2]{0,1:T(2,128)S(1)}, s32[256,2]{0,1:T(2,128)}, u32[]{:S(2)}) copy-start(s32[256,2]{0,1:T(2,128)} %param.31) | copy-start | bytes 6148
  145.9 4.0 %copy-start.4 = (bf16[2048]{0:T(1024)(128)(2,1)S(1)}, bf16[2048]{0:T(1024)(128)(2,1)}, u32[]{:S(2)}) copy-start(bf16[2048]{0:T(1024)(128)(2,1)} %param.29) | copy-start | bytes 12292
  145.9 4.0 %copy-start.5 = (bf16[2048]{0:T(1024)(128)(2,1)S(1)}, bf16[2048]{0:T(1024)(128)(2,1)}, u32[]{:S(2)}) copy-start(bf16[2048]{0:T(1024)(128)(2,1)} %param.30) | copy-start | bytes 12292
  145.9 31.7 %copy-start.3 = (bf16[64,2048]{1,0:T(8,128)(2,1)S(1)}, bf16[64,2048]{1,0:T(8,128)(2,1)}, u32[]{:S(2)}) copy-start(bf16[64,2048]{1,0:T(8,128)(2,1)} %param.19) | copy-start | bytes 786436
  178.9 0.7 copy-start.2
  180.5 8.8 %all-to-all-start = ((bf16[64,4,512]{2,0,1:T(8,128)(2,1)}), bf16[64,4,512]{2,0,1:T(8,128)(2,1)S(1)}, u32[]{:S(2)}, u32[]{:S(2)}) async-start(bf16[64,4,512]{2,0,1:T(8,128)(2,1)} %bitcast.96), calls=%async_computation.1 | async-start | bytes 524288 | tf_op jit(solution)/shard_map/all_to_all | solution.py:159
  183.9 68.5 %all-gather.14.cloned.1.call-start = ((), (), s32[]{:S(2)}) async-start(), calls=%async_computation.11 | async-start | bytes 3276800 | tf_op jit(solution)/shard_map/all_gather | solution.py:164
  215.0 94.9 %reduce-scatter.5.cloned.1.call-start = ((), (), s32[]{:S(2)}) async-start(), calls=%async_computation.12 | async-start | bytes 3276800 | tf_op jit(solution)/shard_map/reduce_scatter | solution.py:173
  256.8 5.7 %copy-start.1 = (bf16[4,640,512]{1,2,0:T(8,128)(2,1)S(1)}, bf16[4,640,512]{1,2,0:T(8,128)(2,1)}, u32[]{:S(2)}) copy-start(bf16[4,640,512]{1,2,0:T(8,128)(2,1)} %copy.90) | copy-start | bytes 7864324
  256.8 5.7 %copy-start.8 = (bf16[1,2048,1024]{2,1,0:T(8,128)(2,1)S(1)}, bf16[1,2048,1024]{2,1,0:T(8,128)(2,1)}, u32[]{:S(2)}) copy-start(bf16[1,2048,1024]{2,1,0:T(8,128)(2,1)} %param.33) | copy-start | bytes 12582916
  262.5 3.5 copy-start.9
  266.0 48.6 %copy-start.7 = (f32[256,2]{0,1:T(2,128)S(1)}, f32[256,2]{0,1:T(2,128)}, u32[]{:S(2)}) copy-start(f32[256,2]{0,1:T(2,128)} %param.32) | copy-start | bytes 6148
  309.9 22.7 %all-to-all-start.2 = ((bf16[512,8,80]{0,2,1:T(8,128)(2,1)}), bf16[512,8,80]{0,2,1:T(8,128)(2,1)S(1)}, u32[]{:S(2)}, u32[]{:S(2)}) async-start(bf16[512,8,80]{0,2,1:T(8,128)(2,1)} %bitcast.110), calls=%async_computation.4 | async-start | bytes 1310720 | tf_op jit(solution)/shard_map/all_to_all | solution.py:181
Sparse Core Ops, SparseCore 0:
  8.9 27.0 all-gather.5
  37.6 23.5 all-gather.7
  62.7 29.3 all-gather.9
  93.6 29.6 all-gather.11
  149.6 26.9 reduce-scatter.2
  215.1 37.2 all-gather.13
  270.3 39.5 reduce-scatter.4
